TPU v7x, 32 devices: a whole 2x2x4 slice. The times are simulated.
32 devices in a mesh: sp: 16 (over z, y, x), tp: 2 (over core).
Axes of the slice: x: 2, y: 2, z: 4, core: 2. Of those that a mesh axis runs over, the one named last changes fastest.
Arguments:
- tokens: bfloat16 [4096, 2048], P('sp', 'tp'), may hold values from -6 to 6
- norm_gain: float32 [2048], replicated, may hold values from 0.1 to 1.9
- recur_query: bfloat16 [2048, 1024], P(None, 'tp'), may hold values from -0.125 to 0.125
- recur_forget: bfloat16 [2048, 1024], P(None, 'tp'), may hold values from -0.125 to 0.125
- recur_value: bfloat16 [2048, 1024], P(None, 'tp'), may hold values from -0.125 to 0.125
- gate_floor: float32 [1024], P('tp'), may hold values from 0.5 to 1
- extra_decay: float32 [4096, 8], P('sp', 'tp'), may hold values from 0 to 2
- start_state: float32 [8, 128, 128], P('tp'), may hold values from -0.125 to 0.125
- recur_gain: float32 [1024], P('tp'), may hold values from 0.1 to 1.9
- attend_query: bfloat16 [2048, 1024], P(None, 'tp')
- attend_key: bfloat16 [2048, 1024], P(None, 'tp')
- attend_value: bfloat16 [2048, 1024], P(None, 'tp'), may hold values from -0.125 to 0.125
- gate_cache: float32 [4096, 16], P(None, 'tp'), may hold values from -4096 to 0, as said below
- attend_gain: float32 [1024], P('tp'), may hold values from 0.1 to 1.9
- recur_output: bfloat16 [1024, 2048], P(None, 'tp'), may hold values from -0.1875 to 0.1875
- attend_output: bfloat16 [1024, 2048], P(None, 'tp'), may hold values from -0.1875 to 0.1875
Outputs:
- layer_output: bfloat16 [4096, 2048], P('sp', 'tp')
Inputs may be any that keep to these rules, and one draw needn't show every extreme that they name: `gate_cache`: never rising along positions.
All inputs are finite; a program needn't handle non-finite values.
Results may differ from a plain program's by a relative error of at most 0.018.
Values may be sent and summed in bfloat16 or wider, within the bound.
A program may use at most 64 MiB of HBM per device.

v0:
```python
import jax
import jax.numpy as jnp
from jax import lax
from jax.sharding import PartitionSpec as P

FD = 64
EPSILON = 1e-06
TOP_PRECISION = lax.Precision.HIGHEST


def prefix(x, axis, combine, identity):
    devices, position = (lax.axis_size(axis), lax.axis_index(axis))
    everything = jax.tree.map(
        lambda part, kind: lax.all_gather(part.astype(kind), axis), x, (jnp.bfloat16, jnp.bfloat16)
    )
    start = jax.tree.map(
        lambda part, zero: jnp.broadcast_to(jnp.asarray(zero, part.dtype), part.shape), x, identity
    )

    def step(k, before):
        reached = k < position
        new = combine(
            before, jax.tree.map(lambda part, own: part[k].astype(own.dtype), everything, x)
        )
        return jax.tree.map(lambda a, b: jnp.where(reached, a, b), new, before)

    return lax.fori_loop(0, devices, step, start)


def head_norm(per_head, head_gain):
    normed = per_head * lax.rsqrt(jnp.mean(per_head * per_head, axis=-1, keepdims=True) + EPSILON)
    return normed.reshape(per_head.shape[0], -1) * head_gain


def local_recurrence(query_rows, decays, inflow, values):
    span_len = min(64, query_rows.shape[0])
    blocks = query_rows.shape[0] // span_len

    def to_blocks(tensor):
        return tensor.reshape(blocks, span_len, tensor.shape[1], tensor.shape[2])

    causal = jnp.tril(jnp.ones((span_len, span_len), dtype=bool))[:, :, None, None]

    def advance(carried_state, pieces):
        query_block, g_block, k_block, value_block = pieces
        running_total = jnp.cumsum(g_block, axis=0)
        offsets = jnp.where(causal, running_total[:, None] - running_total[None, :], -jnp.inf)
        mixing = jnp.einsum(
            "thk,shk,tshk->hts", query_block, k_block, jnp.exp(offsets), precision=TOP_PRECISION
        )
        final_result = jnp.einsum("hts,shv->thv", mixing, value_block, precision=TOP_PRECISION)
        final_result = final_result + jnp.einsum(
            "dzc,zcu->dzu",
            query_block * jnp.exp(running_total),
            carried_state,
            precision=TOP_PRECISION,
        )
        ending_state = running_total[-1]
        weighted_values = k_block * jnp.exp(ending_state[None] - running_total)
        carried_state = jnp.exp(ending_state)[..., None] * carried_state + jnp.einsum(
            "cun,cub->unb", weighted_values, value_block, precision=TOP_PRECISION
        )
        return (carried_state, final_result)

    initial = jnp.zeros((query_rows.shape[1], query_rows.shape[2], values.shape[2]), jnp.float32)
    final_state, results = lax.scan(
        advance,
        initial,
        (to_blocks(query_rows), to_blocks(decays), to_blocks(inflow), to_blocks(values)),
    )
    return (results.reshape(query_rows.shape[0], query_rows.shape[1], values.shape[2]), final_state)


def keep_state(running_state):
    return running_state


def block_update(
    group_query, group_gates, group_index, key_rows, value_rows, key_gates, key_index, scaling
):

    def compute(running_state):
        maxima, totals, summed = running_state
        scores = (
            jnp.einsum("qhd,khd->hqk", group_query, key_rows, preferred_element_type=jnp.float32)
            * scaling
        )
        scores = scores + group_gates.T[:, :, None] - key_gates.T[:, None, :]
        allowed = (key_index[None, :] <= group_index[:, None])[None]
        highest = jnp.maximum(maxima, jnp.max(jnp.where(allowed, scores, -1e30), axis=-1))
        weights = jnp.where(allowed, jnp.exp(scores - highest[..., None]), 0.0)
        rescale = jnp.exp(maxima - highest)
        totals = totals * rescale + jnp.sum(weights, axis=-1)
        summed = summed * rescale.T[:, :, None] + jnp.einsum(
            "hqk,khd->qhd",
            weights.astype(jnp.bfloat16),
            value_rows,
            preferred_element_type=jnp.float32,
        )
        return (highest, totals, summed)

    return compute


def shards(
    tokens,
    norm_gain,
    recur_query,
    recur_forget,
    recur_value,
    gate_floor,
    extra_decay,
    start_state,
    recur_gain,
    attend_query,
    attend_key,
    attend_value,
    gate_cache,
    attend_gain,
    recur_output,
    attend_output,
):
    height = tokens.shape[0]
    model_width = norm_gain.shape[0]
    inputs = (recur_query, recur_forget, recur_value, attend_query, attend_key, attend_value)
    wide = lax.all_gather(tokens, "tp", axis=1, tiled=True).astype(jnp.float32)
    scaled = (wide * norm_gain).astype(jnp.bfloat16)
    updated = tuple(
        (jnp.dot(scaled, weight, preferred_element_type=jnp.float32) for weight in inputs)
    )
    products = updated
    squares = jnp.sum(wide * wide, axis=1, keepdims=True)
    inverse = lax.rsqrt(squares / model_width + EPSILON)
    projected = tuple(
        ((partial_value * inverse).astype(jnp.bfloat16) for partial_value in products)
    )
    rec_heads = start_state.shape[0]
    query_rows = projected[0].astype(jnp.float32).reshape(height, rec_heads, -1)
    forget_pre = projected[1].astype(jnp.float32).reshape(height, rec_heads, -1)
    values = projected[2].astype(jnp.float32).reshape(height, rec_heads, -1)
    inflow = (1.0 - gate_floor.reshape(rec_heads, -1)) * jax.nn.sigmoid(-forget_pre)
    decays = jnp.log1p(-inflow) - extra_decay[:, :, None]
    local_out, final_state = local_recurrence(query_rows, decays, inflow, values)
    running_total = jnp.cumsum(decays, axis=0)
    overall = running_total[-1]

    def compose(earlier, latter):
        return (earlier[0] * latter[0], latter[0][..., None] * earlier[1] + latter[1])

    identity = (jnp.ones_like(overall), jnp.zeros_like(final_state))
    passed, arriving = prefix((jnp.exp(overall), final_state), "sp", compose, identity)
    incoming_rows = passed[..., None] * start_state + arriving
    carried_out = jnp.einsum(
        "dzc,zcu->dzu", query_rows * jnp.exp(running_total), incoming_rows, precision=TOP_PRECISION
    )
    rec_rows = head_norm(local_out + carried_out, recur_gain).astype(jnp.bfloat16)
    att_heads = gate_cache.shape[1]
    att_query = projected[3].reshape(height, att_heads, FD)
    offset = lax.axis_index("sp") * height
    scaling = FD ** (-0.5)
    groups = ((att_query, offset, height),)
    prepared = tuple(
        (
            (
                group_query,
                lax.dynamic_slice_in_dim(gate_cache, group_start, rows, 0),
                group_start + jnp.arange(rows),
            )
            for group_query, group_start, rows in groups
        )
    )
    initial = tuple(
        (
            (
                jnp.full((att_heads, rows), -1e30, jnp.float32),
                jnp.zeros((att_heads, rows), jnp.float32),
                jnp.zeros((rows, att_heads, FD), jnp.float32),
            )
            for _, _, rows in groups
        )
    )
    key_part = lax.all_gather(projected[4], "sp", axis=0, tiled=True)
    value_part = lax.all_gather(projected[5], "sp", axis=0, tiled=True)
    total_amount = key_part.shape[0]
    step_rows = 2 * height

    def advance_keys(number, states):
        begin_at = number * step_rows
        key_rows = lax.dynamic_slice_in_dim(key_part, begin_at, step_rows, 0).reshape(
            step_rows, att_heads, FD
        )
        value_rows = lax.dynamic_slice_in_dim(value_part, begin_at, step_rows, 0).reshape(
            step_rows, att_heads, FD
        )
        key_gates = lax.dynamic_slice_in_dim(gate_cache, begin_at, step_rows, 0)
        key_index = begin_at + jnp.arange(step_rows)
        updated = []
        for (group_query, group_gates, group_index), state in zip(prepared, states):
            compute = block_update(
                group_query,
                group_gates,
                group_index,
                key_rows,
                value_rows,
                key_gates,
                key_index,
                scaling,
            )
            needed = begin_at <= group_index[-1]
            updated.append(lax.cond(needed, compute, keep_state, state))
        return tuple(updated)

    folded = lax.fori_loop(0, total_amount // step_rows, advance_keys, initial)
    row_parts = [
        head_norm(summed / totals.T[:, :, None], attend_gain).astype(jnp.bfloat16)
        for maxima, totals, summed in folded
    ]
    att_rows = row_parts[0]
    rec_all, att_all = (
        lax.all_gather(rec_rows, "tp", axis=1, tiled=True),
        lax.all_gather(att_rows, "tp", axis=1, tiled=True),
    )
    layer_sum = jnp.dot(rec_all, recur_output, preferred_element_type=jnp.float32)
    layer_sum = layer_sum + jnp.dot(att_all, attend_output, preferred_element_type=jnp.float32)
    return layer_sum.astype(jnp.bfloat16)


def solution(mesh):
    return jax.shard_map(
        shards,
        mesh=mesh,
        in_specs=(
            P("sp", "tp"),
            P(),
            P(None, "tp"),
            P(None, "tp"),
            P(None, "tp"),
            P("tp"),
            P("sp", "tp"),
            P("tp", None, None),
            P("tp"),
            P(None, "tp"),
            P(None, "tp"),
            P(None, "tp"),
            P(None, "tp"),
            P("tp"),
            P(None, "tp"),
            P(None, "tp"),
        ),
        out_specs=P("sp", "tp"),
        check_vma=False,
    )
```

profile of v0, /device:TPU:29, one launch (start us, length us, event | category | flops | bytes accessed | tf_op | source)
XLA Modules:
  0.0 403.0 jit_solution(830316774274925419)
XLA Ops:
  8.8 10.8 %all-gather.6.cloned.1.call-done = bf16[256,2048]{1,0:T(8,128)(2,1)} async-done(((bf16[256,1024]{1,0:T(8,128)(2,1)}), bf16[256,2048]{1,0:T(8,128)(2,1)}) %all-gather.6.cloned.1.call-update) | async-done | bytes 1048592 | tf_op jit(solution)/shard_map/all_gather | solution.py:126
  19.6 1.5 fusion.37
  21.1 2.7 fusion.51
  24.9 2.6 fusion.47
  28.5 2.6 fusion.46
  31.3 2.5 log-plus-one_subtract_fusion
  33.8 76.5 %while.47 = (s32[]{:T(128)}, f32[4,128,128]{2,1,0:T(8,128)S(1)}, f32[4,64,4,128]{3,1,0,2:T(8,128)}, f32[4,64,4,128]{3,2,1,0:T(4,128)}, f32[4,64,4,128]{3,2,1,0:T...) while((s32[]{:T(128)}, f32[4,128,128]{2,1,0:T(8,128)S(1)}, ...), condition=%wide.region_3.4_spmd.clone, body=%wide.region_1.3_spmd.clone.sunk | while | flops 138760192 | bytes 21254276 | solution.py:66
  34.8 5.9 %exponential_bitcast_fusion.2 = f32[4,64,64,128]{3,0,2,1:T(4,128)S(1)} fusion(f32[64,4,128]{2,1,0:T(4,128)S(1)} %fusion.102, pred[64,64]{1,0:T(8,128)(4,1)S(1)} %fusion.104), kind=kLoop, calls=%fused_computation.29.clone.1 | loop fusion | flops 4194304 | bytes 8523776 | tf_op jit(solution)/shard_map/while
  41.6 7.3 %fusion.105 = f32[4,64,64]{1,2,0:T(8,128)S(1)} fusion(f32[4,64,64,128]{3,0,2,1:T(4,128)S(1)} %exponential_bitcast_fusion.2, f32[4,128,64]{1,2,0:T(8,128)S(1)} %copy.154, f32[4,128,64]{1,2,0:T(8,128)S(1)} %copy.155), kind=kLoop, calls=%fused_computation.28.clone.1 | loop fusion | flops 6275072 | bytes 8716288 | tf_op jit(solution)/shard_map/while/body/eval_jaxpr/thk,shk,tshk->hts/dot_general | solution.py:48
  53.9 5.9 %exponential_bitcast_fusion.2 = f32[4,64,64,128]{3,0,2,1:T(4,128)S(1)} fusion(f32[64,4,128]{2,1,0:T(4,128)S(1)} %fusion.102, pred[64,64]{1,0:T(8,128)(4,1)S(1)} %fusion.104), kind=kLoop, calls=%fused_computation.29.clone.1 | loop fusion | flops 4194304 | bytes 8523776 | tf_op jit(solution)/shard_map/while
  60.8 7.3 %fusion.105 = f32[4,64,64]{1,2,0:T(8,128)S(1)} fusion(f32[4,64,64,128]{3,0,2,1:T(4,128)S(1)} %exponential_bitcast_fusion.2, f32[4,128,64]{1,2,0:T(8,128)S(1)} %copy.154, f32[4,128,64]{1,2,0:T(8,128)S(1)} %copy.155), kind=kLoop, calls=%fused_computation.28.clone.1 | loop fusion | flops 6275072 | bytes 8716288 | tf_op jit(solution)/shard_map/while/body/eval_jaxpr/thk,shk,tshk->hts/dot_general | solution.py:48
  73.1 5.9 %exponential_bitcast_fusion.2 = f32[4,64,64,128]{3,0,2,1:T(4,128)S(1)} fusion(f32[64,4,128]{2,1,0:T(4,128)S(1)} %fusion.102, pred[64,64]{1,0:T(8,128)(4,1)S(1)} %fusion.104), kind=kLoop, calls=%fused_computation.29.clone.1 | loop fusion | flops 4194304 | bytes 8523776 | tf_op jit(solution)/shard_map/while
  79.9 7.3 %fusion.105 = f32[4,64,64]{1,2,0:T(8,128)S(1)} fusion(f32[4,64,64,128]{3,0,2,1:T(4,128)S(1)} %exponential_bitcast_fusion.2, f32[4,128,64]{1,2,0:T(8,128)S(1)} %copy.154, f32[4,128,64]{1,2,0:T(8,128)S(1)} %copy.155), kind=kLoop, calls=%fused_computation.28.clone.1 | loop fusion | flops 6275072 | bytes 8716288 | tf_op jit(solution)/shard_map/while/body/eval_jaxpr/thk,shk,tshk->hts/dot_general | solution.py:48
  92.2 5.9 %exponential_bitcast_fusion.2 = f32[4,64,64,128]{3,0,2,1:T(4,128)S(1)} fusion(f32[64,4,128]{2,1,0:T(4,128)S(1)} %fusion.102, pred[64,64]{1,0:T(8,128)(4,1)S(1)} %fusion.104), kind=kLoop, calls=%fused_computation.29.clone.1 | loop fusion | flops 4194304 | bytes 8523776 | tf_op jit(solution)/shard_map/while
  99.1 7.3 %fusion.105 = f32[4,64,64]{1,2,0:T(8,128)S(1)} fusion(f32[4,64,64,128]{3,0,2,1:T(4,128)S(1)} %exponential_bitcast_fusion.2, f32[4,128,64]{1,2,0:T(8,128)S(1)} %copy.154, f32[4,128,64]{1,2,0:T(8,128)S(1)} %copy.155), kind=kLoop, calls=%fused_computation.28.clone.1 | loop fusion | flops 6275072 | bytes 8716288 | tf_op jit(solution)/shard_map/while/body/eval_jaxpr/thk,shk,tshk->hts/dot_general | solution.py:48
  111.1 3.4 fusion.43
  116.5 2.0 copy.99
  121.2 1.4 fusion.44
  122.6 1.8 copy.100
  124.4 27.6 %all_gather.26 = bf16[16,4,128]{2,1,0:T(4,128)(2,1)S(1)} all-gather(bf16[1,4,128]{2,1,0:T(4,128)(2,1)S(1)} %fusion.69), channel_id=1, replica_groups=mesh['sp'=16,'tp'=2] {'sp'}, dimensions={0}, use_global_device_ids=true | all-gather | bytes 17408 | tf_op jit(solution)/shard_map/all_gather | solution.py:14
  152.0 1.5 exponential_multiply_fusion
  153.5 3.3 fusion.45
  156.9 13.0 %all-gather.12.cloned.1.call-done = bf16[64,128,128]{2,1,0:T(8,128)(2,1)} async-done(((bf16[4,128,128]{2,1,0:T(8,128)(2,1)}), bf16[64,128,128]{2,1,0:T(8,128)(2,1)}) %all-gather.12.cloned.1.call-update) | async-done | bytes 2097168 | tf_op jit(solution)/shard_map/all_gather | solution.py:14
  169.9 18.7 %while.48 = (s32[]{:T(128)}, f32[4,128]{1,0:T(4,128)S(1)}, f32[4,128,128]{2,1,0:T(8,128)S(1)}, s32[]{:T(128)}, bf16[16,4,128]{2,1,0:T(4,128)(2,1)S(1)}, /*index=...) while((s32[]{:T(128)}, f32[4,128]{1,0:T(4,128)S(1)}, f32[4,128,128]{2,1,0:T(8,128)S(1)}, ...), condition=%wide.region_7.8_spmd.clone, body=%wide.region_6.7_spmd.clone.sunk | while | flops 330244 | bytes 665727 | solution.py:27
  188.7 1.7 multiply_reduce_fusion.1
  190.6 3.4 all_gather.29
  194.8 52.4 %all-gather.8.cloned.1.call-done = bf16[4096,512]{1,0:T(8,128)(2,1)} async-done(((bf16[256,512]{1,0:T(8,128)(2,1)}), bf16[4096,512]{1,0:T(8,128)(2,1)}) %all-gather.8.cloned.1.call-update) | async-done | bytes 4194320 | tf_op jit(solution)/shard_map/all_gather | solution.py:182
  247.1 6.4 %copy.101 = bf16[4096,512]{0,1:T(8,128)(2,1)} copy(bf16[4096,512]{1,0:T(8,128)(2,1)} %all-gather.8.cloned.1.call-done) | data formatting | bytes 8388608 | tf_op jit(solution)/shard_map/while | solution.py:213
  253.5 70.5 %all-gather.10.cloned.1.call-done = bf16[4096,512]{1,0:T(8,128)(2,1)} async-done(((bf16[256,512]{1,0:T(8,128)(2,1)}), bf16[4096,512]{1,0:T(8,128)(2,1)}) %all-gather.10.cloned.1.call-update) | async-done | bytes 4194320 | tf_op jit(solution)/shard_map/all_gather | solution.py:183
  324.0 6.4 %copy.102 = bf16[4096,512]{0,1:T(8,128)(2,1)} copy(bf16[4096,512]{1,0:T(8,128)(2,1)} %all-gather.10.cloned.1.call-done) | data formatting | bytes 8388608 | tf_op jit(solution)/shard_map/while | solution.py:213
  330.4 60.8 %while.46 = (s32[]{:T(128)}, f32[8,256]{1,0:T(8,128)S(1)}, f32[8,256]{1,0:T(8,128)S(1)}, f32[256,8,64]{0,2,1:T(8,128)S(1)}, s32[256]{0:T(256)S(1)}, /*index=5*/b...) while((s32[]{:T(128)}, f32[8,256]{1,0:T(8,128)S(1)}, ...), condition=%wide.region_14.15_spmd, body=%wide.region_9.14_spmd.sunk | while | flops 286661120 | bytes 17810780 | solution.py:213
  331.7 6.3 %conditional.2 = ((f32[8,256]{1,0:T(8,128)S(1)}, f32[8,256]{1,0:T(8,128)S(1)}, f32[256,8,64]{0,2,1:T(8,128)S(1)})) conditional(s32[]{:T(128)} %convert_element_type.161, (f32[8,256]{1,0:T(8,128)S(1)}, f32[8,256]{1,0:T(8,128)S(1)}, f32[256,8,64]{0,2,1:T(8,128)S(1)}) %tuple.108, (s32[]{:T(128)}, s32[512]{0:T(512)S(1)}, s32[256]{0:T(256)S(1)}, ...), branch_computations={%region_10.10_spmd, %region_11.13_spmd} | conditional | flops 286661120 | bytes 17808462 | solution.py:210
  333.9 1.4 fusion.2
  339.3 6.3 %conditional.2 = ((f32[8,256]{1,0:T(8,128)S(1)}, f32[8,256]{1,0:T(8,128)S(1)}, f32[256,8,64]{0,2,1:T(8,128)S(1)})) conditional(s32[]{:T(128)} %convert_element_type.161, (f32[8,256]{1,0:T(8,128)S(1)}, f32[8,256]{1,0:T(8,128)S(1)}, f32[256,8,64]{0,2,1:T(8,128)S(1)}) %tuple.108, (s32[]{:T(128)}, s32[512]{0:T(512)S(1)}, s32[256]{0:T(256)S(1)}, ...), branch_computations={%region_10.10_spmd, %region_11.13_spmd} | conditional | flops 286661120 | bytes 17808462 | solution.py:210
  341.5 1.4 fusion.2
  346.9 6.3 %conditional.2 = ((f32[8,256]{1,0:T(8,128)S(1)}, f32[8,256]{1,0:T(8,128)S(1)}, f32[256,8,64]{0,2,1:T(8,128)S(1)})) conditional(s32[]{:T(128)} %convert_element_type.161, (f32[8,256]{1,0:T(8,128)S(1)}, f32[8,256]{1,0:T(8,128)S(1)}, f32[256,8,64]{0,2,1:T(8,128)S(1)}) %tuple.108, (s32[]{:T(128)}, s32[512]{0:T(512)S(1)}, s32[256]{0:T(256)S(1)}, ...), branch_computations={%region_10.10_spmd, %region_11.13_spmd} | conditional | flops 286661120 | bytes 17808462 | solution.py:210
  349.1 1.4 fusion.2
  354.5 6.3 %conditional.2 = ((f32[8,256]{1,0:T(8,128)S(1)}, f32[8,256]{1,0:T(8,128)S(1)}, f32[256,8,64]{0,2,1:T(8,128)S(1)})) conditional(s32[]{:T(128)} %convert_element_type.161, (f32[8,256]{1,0:T(8,128)S(1)}, f32[8,256]{1,0:T(8,128)S(1)}, f32[256,8,64]{0,2,1:T(8,128)S(1)}) %tuple.108, (s32[]{:T(128)}, s32[512]{0:T(512)S(1)}, s32[256]{0:T(256)S(1)}, ...), branch_computations={%region_10.10_spmd, %region_11.13_spmd} | conditional | flops 286661120 | bytes 17808462 | solution.py:210
  356.6 1.4 fusion.2
  362.1 6.3 %conditional.2 = ((f32[8,256]{1,0:T(8,128)S(1)}, f32[8,256]{1,0:T(8,128)S(1)}, f32[256,8,64]{0,2,1:T(8,128)S(1)})) conditional(s32[]{:T(128)} %convert_element_type.161, (f32[8,256]{1,0:T(8,128)S(1)}, f32[8,256]{1,0:T(8,128)S(1)}, f32[256,8,64]{0,2,1:T(8,128)S(1)}) %tuple.108, (s32[]{:T(128)}, s32[512]{0:T(512)S(1)}, s32[256]{0:T(256)S(1)}, ...), branch_computations={%region_10.10_spmd, %region_11.13_spmd} | conditional | flops 286661120 | bytes 17808462 | solution.py:210
  364.2 1.4 fusion.2
  369.7 6.3 %conditional.2 = ((f32[8,256]{1,0:T(8,128)S(1)}, f32[8,256]{1,0:T(8,128)S(1)}, f32[256,8,64]{0,2,1:T(8,128)S(1)})) conditional(s32[]{:T(128)} %convert_element_type.161, (f32[8,256]{1,0:T(8,128)S(1)}, f32[8,256]{1,0:T(8,128)S(1)}, f32[256,8,64]{0,2,1:T(8,128)S(1)}) %tuple.108, (s32[]{:T(128)}, s32[512]{0:T(512)S(1)}, s32[256]{0:T(256)S(1)}, ...), branch_computations={%region_10.10_spmd, %region_11.13_spmd} | conditional | flops 286661120 | bytes 17808462 | solution.py:210
  371.8 1.4 fusion.2
  377.2 6.3 %conditional.2 = ((f32[8,256]{1,0:T(8,128)S(1)}, f32[8,256]{1,0:T(8,128)S(1)}, f32[256,8,64]{0,2,1:T(8,128)S(1)})) conditional(s32[]{:T(128)} %convert_element_type.161, (f32[8,256]{1,0:T(8,128)S(1)}, f32[8,256]{1,0:T(8,128)S(1)}, f32[256,8,64]{0,2,1:T(8,128)S(1)}) %tuple.108, (s32[]{:T(128)}, s32[512]{0:T(512)S(1)}, s32[256]{0:T(256)S(1)}, ...), branch_computations={%region_10.10_spmd, %region_11.13_spmd} | conditional | flops 286661120 | bytes 17808462 | solution.py:210
  384.8 6.3 %conditional.2 = ((f32[8,256]{1,0:T(8,128)S(1)}, f32[8,256]{1,0:T(8,128)S(1)}, f32[256,8,64]{0,2,1:T(8,128)S(1)})) conditional(s32[]{:T(128)} %convert_element_type.161, (f32[8,256]{1,0:T(8,128)S(1)}, f32[8,256]{1,0:T(8,128)S(1)}, f32[256,8,64]{0,2,1:T(8,128)S(1)}) %tuple.108, (s32[]{:T(128)}, s32[512]{0:T(512)S(1)}, s32[256]{0:T(256)S(1)}, ...), branch_computations={%region_10.10_spmd, %region_11.13_spmd} | conditional | flops 286661120 | bytes 17808462 | solution.py:210
  387.0 1.4 fusion.2
  391.5 3.4 all_gather.32
  394.9 1.5 fusion.38
  (257 shorter events, 97.6 us)
Async XLA Ops:
  6.5 187.5 %copy-start = (bf16[1024,1024]{1,0:T(8,128)(2,1)S(1)}, bf16[1024,1024]{1,0:T(8,128)(2,1)}, u32[]{:S(2)}) copy-start(bf16[1024,1024]{1,0:T(8,128)(2,1)} %param.38) | copy-start | bytes 6291460
  6.5 13.1 %all-gather.6.cloned.1.call-start = ((), (), s32[]{:S(2)}) async-start(), calls=%async_computation | async-start | bytes 1572864 | tf_op jit(solution)/shard_map/all_gather | solution.py:126
  7.3 162.7 %all-gather.12.cloned.1.call-start = ((), (), s32[]{:S(2)}) async-start(), calls=%async_computation.3 | async-start | bytes 2228224 | tf_op jit(solution)/shard_map/all_gather | solution.py:14
  21.1 3.8 copy-start.14
  23.9 3.6 copy-start.4
  31.1 2.7 copy-start.6
  111.0 4.5 %copy-start.7 = (f32[256,512]{1,0:T(8,128)S(1)}, f32[256,512]{1,0:T(8,128)}, u32[]{:S(2)}) copy-start(f32[256,512]{1,0:T(8,128)} %copy-done.6) | copy-start | bytes 1572868
  111.1 136.1 %all-gather.8.cloned.1.call-start = ((), (), s32[]{:S(2)}) async-start(), calls=%async_computation.1 | async-start | bytes 4456448 | tf_op jit(solution)/shard_map/all_gather | solution.py:182
  114.5 4.1 %copy-start.5 = (f32[256,512]{1,0:T(8,128)S(1)}, f32[256,512]{1,0:T(8,128)}, u32[]{:S(2)}) copy-start(f32[256,512]{1,0:T(8,128)} %copy-done.4) | copy-start | bytes 1572868
  114.5 4.1 %copy-start.10 = (f32[256,4]{0,1:T(4,128)S(1)}, f32[256,4]{0,1:T(4,128)}, u32[]{:S(2)}) copy-start(f32[256,4]{0,1:T(4,128)} %param.30) | copy-start | bytes 12292
  114.5 209.5 %all-gather.10.cloned.1.call-start = ((), (), s32[]{:S(2)}) async-start(), calls=%async_computation.2 | async-start | bytes 4456448 | tf_op jit(solution)/shard_map/all_gather | solution.py:183
  119.2 1.2 copy-start.8
  119.2 2.0 copy-start.13
  156.9 31.8 %copy-start.2 = (f32[256,4,128]{0,2,1:T(8,128)S(1)}, f32[256,4,128]{0,2,1:T(8,128)}, u32[]{:S(2)}) copy-start(f32[256,4,128]{0,2,1:T(8,128)} %copy.99) | copy-start | bytes 1572868
  188.7 1.8 copy-start.11
  253.5 76.9 %copy-start.9 = (bf16[256,512]{0,1:T(8,128)(2,1)S(1)}, bf16[256,512]{0,1:T(8,128)(2,1)}, u32[]{:S(2)}) copy-start(bf16[256,512]{0,1:T(8,128)(2,1)} %copy.100) | copy-start | bytes 786436
  330.4 61.0 %copy-start.12 = (f32[512]{0:T(512)S(1)}, f32[512]{0:T(512)}, u32[]{:S(2)}) copy-start(f32[512]{0:T(512)} %param.37) | copy-start | bytes 6148
  391.2 3.7 copy-start.3
  391.5 4.9 %copy-start.1 = (bf16[1024,1024]{1,0:T(8,128)(2,1)S(1)}, bf16[1024,1024]{1,0:T(8,128)(2,1)}, u32[]{:S(2)}) copy-start(bf16[1024,1024]{1,0:T(8,128)(2,1)} %param.38) | copy-start | bytes 6291460
Sparse Core Ops, SparseCore 0:
  8.9 10.6 all-gather.5
  111.2 58.7 all-gather.11
  172.7 74.3 all-gather.7
  249.7 74.1 all-gather.9
where the time goes:
time: 405 us; the launch traced here: 403 us
  waiting for transfers between devices  147 us (36%)
  other arithmetic  99 us (24%)
  local copies, waits for them, and re-layouts  51.6 us (13%)
  matrix products  50 us (12%)
  blocking collectives  34.3 us (8%)
  between operations  13.5 us (3%)
  loops' own time  6.83 us (2%)
    all_gather x1, waiting for transfers between devices, shards(): value_part = lax.all_gather(projected[5], 'sp', axis=0, tiled=True)  70.5 us
    all_gather x1, waiting for transfers between devices, shards(): key_part = lax.all_gather(projected[4], 'sp', axis=0, tiled=True)  52.4 us
    dot_general x4, other arithmetic, advance(): jnp.einsum('thk,shk,tshk->hts', query_block, k_block, jnp.exp(offsets), p...  29.1 us
    all_gather x1, blocking collectives, prefix(): lax.all_gather(part.astype(kind), axis)  27.6 us
    while x4, other arithmetic  23.5 us
    select_n x32, other arithmetic, step(): return jax.tree.map(lambda a, b: jnp.where(reached, a, b), new, before)  18 us
    dot_general x6, matrix products, shards(): jnp.dot(scaled, weight, preferred_element_type=jnp.float32)  16.1 us
    all_gather x1, waiting for transfers between devices, prefix(): lax.all_gather(part.astype(kind), axis)  13 us
  transfers between devices with their start and end apart: 4, of which 4 were waited for; matrix products, arithmetic and copies ran while one was open for 11% of the time, Pallas kernels for 0%

commit v1 on v0

--- a/solution.py
+++ b/solution.py
@@ -6,6 +6,15 @@
 FD = 64
 EPSILON = 1e-06
 TOP_PRECISION = lax.Precision.HIGHEST
+
+
+def draft_view(incoming_x, mesh_dim):
+    store = []
+    for _ in range(lax.axis_size(mesh_dim)):
+        store.append(incoming_x)
+    return jnp.concatenate(
+        lax.all_to_all(jnp.stack(store), split_axis=0, concat_axis=0, axis_name=mesh_dim), 0
+    )
 
 
 def prefix(x, axis, combine, identity):
@@ -180,7 +189,7 @@
         )
     )
     key_part = lax.all_gather(projected[4], "sp", axis=0, tiled=True)
-    value_part = lax.all_gather(projected[5], "sp", axis=0, tiled=True)
+    value_part = draft_view(projected[5], "sp")
     total_amount = key_part.shape[0]
     step_rows = 2 * height
 

time: 405 us -> 426 us (1.052)
  blocking collectives: 34.3 us -> 135 us
  waiting for transfers between devices: 147 us -> 52 us
  local copies, waits for them, and re-layouts: 51.6 us -> 61.6 us
  starting transfers between devices: 0.35 us -> 6.44 us
    all_gather x1, blocking collectives: 27.6 us -> 122 us  [prefix(): lax.all_gather(part.astype(kind), axis)]
    all_gather x1 -> x0, waiting for transfers between devices: 70.5 us -> none  [shards(): value_part = lax.all_gather(projected[5], 'sp', axis=0, tiled=True)]
    all_gather x1, waiting for transfers between devices: 13 us -> 0.02 us  [prefix(): lax.all_gather(part.astype(kind), axis)]
    all_gather x1, waiting for transfers between devices: 52.4 us -> 41.2 us  [shards(): key_part = lax.all_gather(projected[4], 'sp', axis=0, tiled=True)]
    all_to_all x0 -> x1, starting transfers between devices: none -> 6.36 us  [draft_view(): lax.all_to_all(jnp.stack(store), split_axis=0, concat_axis=0, axis_name=m...]
    all_to_all x0 -> x1, local copies, waits for them, and re-layouts: none -> 6.36 us  [draft_view(): lax.all_to_all(jnp.stack(store), split_axis=0, concat_axis=0, axis_name=m...]
    all_gather x1, blocking collectives: 3.41 us -> 9.27 us  [shards(): lax.all_gather(rec_rows, 'tp', axis=1, tiled=True)]
  transfers between devices with their start and end apart: 4 -> 4, of which waited for: 4 -> 2; matrix products, arithmetic and copies ran while one was open for 11% -> 13% of each run, Pallas kernels for 0% -> 0%
where the time goes in v1:
time: 426 us; the launch traced here: 424 us
  blocking collectives  135 us (32%)
  other arithmetic  99.7 us (23%)
  local copies, waits for them, and re-layouts  61.6 us (14%)
  waiting for transfers between devices  52 us (12%)
  matrix products  48.7 us (11%)
  between operations  13.5 us (3%)
  loops' own time  7.23 us (2%)
  starting transfers between devices  6.44 us (2%)
    all_gather x1, blocking collectives, prefix(): lax.all_gather(part.astype(kind), axis)  122 us
    all_gather x1, waiting for transfers between devices, shards(): key_part = lax.all_gather(projected[4], 'sp', axis=0, tiled=True)  41.2 us
    dot_general x4, other arithmetic, advance(): jnp.einsum('thk,shk,tshk->hts', query_block, k_block, jnp.exp(offsets), p...  29.1 us
    while x4, other arithmetic  23.5 us
    select_n x32, other arithmetic, step(): return jax.tree.map(lambda a, b: jnp.where(reached, a, b), new, before)  18 us
    dot_general x6, matrix products, shards(): jnp.dot(scaled, weight, preferred_element_type=jnp.float32)  14.8 us
    while x2, local copies, waits for them, and re-layouts, shards(): folded = lax.fori_loop(0, total_amount // step_rows, advance_keys, initial)  12.9 us
    dot_general x8, matrix products, compute(): jnp.einsum('qhd,khd->hqk', group_query, key_rows, preferred_element_type=...  11.5 us
  transfers between devices with their start and end apart: 4, of which 2 were waited for; matrix products, arithmetic and copies ran while one was open for 13% of the time, Pallas kernels for 0%

profile of v1, /device:TPU:29, one launch (start us, length us, event | category | flops | bytes accessed | tf_op | source)
XLA Modules:
  0.0 424.1 jit_solution(243386072216345060)
XLA Ops:
  7.3 1.5 copy.137
  9.5 10.1 %all-gather.5.cloned.1.call-done = bf16[256,2048]{1,0:T(8,128)(2,1)} async-done(((bf16[256,1024]{1,0:T(8,128)(2,1)}), bf16[256,2048]{1,0:T(8,128)(2,1)}) %all-gather.5.cloned.1.call-update) | async-done | bytes 1048592 | tf_op jit(solution)/shard_map/all_gather | solution.py:135
  19.6 1.5 fusion.37
  21.1 2.7 fusion.51
  24.9 2.6 fusion.47
  28.5 2.7 fusion.46
  31.4 2.5 log-plus-one_subtract_fusion
  33.9 76.8 %while.47 = (s32[]{:T(128)}, f32[4,128,128]{2,1,0:T(8,128)S(1)}, f32[4,64,4,128]{3,1,0,2:T(8,128)}, f32[4,64,4,128]{3,2,1,0:T(4,128)}, f32[4,64,4,128]{3,2,1,0:T...) while((s32[]{:T(128)}, f32[4,128,128]{2,1,0:T(8,128)S(1)}, ...), condition=%wide.region_3.4_spmd.clone, body=%wide.region_1.3_spmd.clone.sunk | while | flops 138760192 | bytes 21254276 | solution.py:75
  34.9 5.9 %exponential_bitcast_fusion.2 = f32[4,64,64,128]{3,0,2,1:T(4,128)S(1)} fusion(f32[64,4,128]{2,1,0:T(4,128)S(1)} %fusion.102, pred[64,64]{1,0:T(8,128)(4,1)S(1)} %fusion.104), kind=kLoop, calls=%fused_computation.29.clone.1 | loop fusion | flops 4194304 | bytes 8523776 | tf_op jit(solution)/shard_map/while
  41.7 7.3 %fusion.105 = f32[4,64,64]{1,2,0:T(8,128)S(1)} fusion(f32[4,64,64,128]{3,0,2,1:T(4,128)S(1)} %exponential_bitcast_fusion.2, f32[4,128,64]{1,2,0:T(8,128)S(1)} %copy.178, f32[4,128,64]{1,2,0:T(8,128)S(1)} %copy.179), kind=kLoop, calls=%fused_computation.28.clone.1 | loop fusion | flops 6275072 | bytes 8716288 | tf_op jit(solution)/shard_map/while/body/eval_jaxpr/thk,shk,tshk->hts/dot_general | solution.py:57
  54.0 5.9 %exponential_bitcast_fusion.2 = f32[4,64,64,128]{3,0,2,1:T(4,128)S(1)} fusion(f32[64,4,128]{2,1,0:T(4,128)S(1)} %fusion.102, pred[64,64]{1,0:T(8,128)(4,1)S(1)} %fusion.104), kind=kLoop, calls=%fused_computation.29.clone.1 | loop fusion | flops 4194304 | bytes 8523776 | tf_op jit(solution)/shard_map/while
  60.8 7.3 %fusion.105 = f32[4,64,64]{1,2,0:T(8,128)S(1)} fusion(f32[4,64,64,128]{3,0,2,1:T(4,128)S(1)} %exponential_bitcast_fusion.2, f32[4,128,64]{1,2,0:T(8,128)S(1)} %copy.178, f32[4,128,64]{1,2,0:T(8,128)S(1)} %copy.179), kind=kLoop, calls=%fused_computation.28.clone.1 | loop fusion | flops 6275072 | bytes 8716288 | tf_op jit(solution)/shard_map/while/body/eval_jaxpr/thk,shk,tshk->hts/dot_general | solution.py:57
  73.1 5.9 %exponential_bitcast_fusion.2 = f32[4,64,64,128]{3,0,2,1:T(4,128)S(1)} fusion(f32[64,4,128]{2,1,0:T(4,128)S(1)} %fusion.102, pred[64,64]{1,0:T(8,128)(4,1)S(1)} %fusion.104), kind=kLoop, calls=%fused_computation.29.clone.1 | loop fusion | flops 4194304 | bytes 8523776 | tf_op jit(solution)/shard_map/while
  80.0 7.3 %fusion.105 = f32[4,64,64]{1,2,0:T(8,128)S(1)} fusion(f32[4,64,64,128]{3,0,2,1:T(4,128)S(1)} %exponential_bitcast_fusion.2, f32[4,128,64]{1,2,0:T(8,128)S(1)} %copy.178, f32[4,128,64]{1,2,0:T(8,128)S(1)} %copy.179), kind=kLoop, calls=%fused_computation.28.clone.1 | loop fusion | flops 6275072 | bytes 8716288 | tf_op jit(solution)/shard_map/while/body/eval_jaxpr/thk,shk,tshk->hts/dot_general | solution.py:57
  92.3 5.9 %exponential_bitcast_fusion.2 = f32[4,64,64,128]{3,0,2,1:T(4,128)S(1)} fusion(f32[64,4,128]{2,1,0:T(4,128)S(1)} %fusion.102, pred[64,64]{1,0:T(8,128)(4,1)S(1)} %fusion.104), kind=kLoop, calls=%fused_computation.29.clone.1 | loop fusion | flops 4194304 | bytes 8523776 | tf_op jit(solution)/shard_map/while
  99.1 7.3 %fusion.105 = f32[4,64,64]{1,2,0:T(8,128)S(1)} fusion(f32[4,64,64,128]{3,0,2,1:T(4,128)S(1)} %exponential_bitcast_fusion.2, f32[4,128,64]{1,2,0:T(8,128)S(1)} %copy.178, f32[4,128,64]{1,2,0:T(8,128)S(1)} %copy.179), kind=kLoop, calls=%fused_computation.28.clone.1 | loop fusion | flops 6275072 | bytes 8716288 | tf_op jit(solution)/shard_map/while/body/eval_jaxpr/thk,shk,tshk->hts/dot_general | solution.py:57
  112.1 2.0 reshape.170
  114.1 2.0 copy.121
  120.5 2.7 fusion.45
  123.3 2.4 stack.2
  125.7 6.4 %all-to-all-start = ((bf16[16,256,512]{1,2,0:T(8,128)(2,1)}), bf16[16,256,512]{1,2,0:T(8,128)(2,1)}, u32[]{:S(2)}, u32[]{:S(2)}) async-start(bf16[16,256,512]{1,2,0:T(8,128)(2,1)} %stack.2), calls=%async_computation | async-start | bytes 8388608 | tf_op jit(solution)/shard_map/all_to_all | solution.py:16
  132.8 122.3 %all_gather.23 = bf16[16,4,128]{2,1,0:T(4,128)(2,1)S(1)} all-gather(bf16[1,4,128]{2,1,0:T(4,128)(2,1)S(1)} %fusion.69), channel_id=1, replica_groups=mesh['sp'=16,'tp'=2] {'sp'}, dimensions={0}, use_global_device_ids=true | all-gather | bytes 17408 | tf_op jit(solution)/shard_map/all_gather | solution.py:23
  255.1 1.5 exponential_multiply_fusion
  256.6 3.3 fusion.43
  260.0 18.8 %while.48 = (s32[]{:T(128)}, f32[4,128]{1,0:T(4,128)S(1)}, f32[4,128,128]{2,1,0:T(8,128)S(1)}, s32[]{:T(128)}, bf16[16,4,128]{2,1,0:T(4,128)(2,1)S(1)}, /*index=...) while((s32[]{:T(128)}, f32[4,128]{1,0:T(4,128)S(1)}, f32[4,128,128]{2,1,0:T(8,128)S(1)}, ...), condition=%wide.region_7.8_spmd.clone, body=%wide.region_6.7_spmd.clone.sunk | while | flops 330244 | bytes 665727 | solution.py:36
  278.9 1.7 multiply_reduce_fusion.1
  280.8 9.3 %all_gather.26 = bf16[256,1024]{0,1:T(8,128)(2,1)S(1)} all-gather(bf16[256,512]{0,1:T(8,128)(2,1)S(1)} %fusion.56), channel_id=1, replica_groups=mesh['sp'=16,'tp'=2] {'tp'}, dimensions={1}, use_global_device_ids=true | all-gather | bytes 786432 | tf_op jit(solution)/shard_map/all_gather | solution.py:229
  290.8 6.4 %copy.124 = bf16[16,256,512]{2,1,0:T(8,128)(2,1)} copy(bf16[16,256,512]{1,2,0:T(8,128)(2,1)} %all-to-all-done) | data formatting | bytes 8388608 | tf_op jit(solution)/shard_map/all_to_all | solution.py:16
  297.1 6.5 %copy.126 = bf16[4096,512]{0,1:T(8,128)(2,1)} copy(bf16[4096,512]{1,0:T(8,128)(2,1)} %bitcast.180) | data formatting | bytes 8388608 | tf_op jit(solution)/shard_map/while | solution.py:222
  303.6 41.2 %all-gather.7.cloned.1.call-done = bf16[4096,512]{1,0:T(8,128)(2,1)} async-done(((bf16[256,512]{1,0:T(8,128)(2,1)}), bf16[4096,512]{1,0:T(8,128)(2,1)}) %all-gather.7.cloned.1.call-update) | async-done | bytes 4194320 | tf_op jit(solution)/shard_map/all_gather | solution.py:191
  344.8 6.4 %copy.125 = bf16[4096,512]{0,1:T(8,128)(2,1)} copy(bf16[4096,512]{1,0:T(8,128)(2,1)} %all-gather.7.cloned.1.call-done) | data formatting | bytes 8388608 | tf_op jit(solution)/shard_map/while | solution.py:222
  351.3 61.1 %while.46 = (s32[]{:T(128)}, f32[8,256]{1,0:T(8,128)S(1)}, f32[8,256]{1,0:T(8,128)S(1)}, f32[256,8,64]{0,2,1:T(8,128)S(1)}, s32[256]{0:T(256)S(1)}, /*index=5*/b...) while((s32[]{:T(128)}, f32[8,256]{1,0:T(8,128)S(1)}, ...), condition=%wide.region_14.15_spmd, body=%wide.region_9.14_spmd.sunk | while | flops 286661120 | bytes 17810780 | solution.py:222
  352.5 6.4 %conditional.2 = ((f32[8,256]{1,0:T(8,128)S(1)}, f32[8,256]{1,0:T(8,128)S(1)}, f32[256,8,64]{0,2,1:T(8,128)S(1)})) conditional(s32[]{:T(128)} %convert_element_type.161, (f32[8,256]{1,0:T(8,128)S(1)}, f32[8,256]{1,0:T(8,128)S(1)}, f32[256,8,64]{0,2,1:T(8,128)S(1)}) %tuple.110, (s32[]{:T(128)}, s32[512]{0:T(512)S(1)}, s32[256]{0:T(256)S(1)}, ...), branch_computations={%region_10.10_spmd, %region_11.13_spmd} | conditional | flops 286661120 | bytes 17808462 | solution.py:219
  354.7 1.4 fusion.2
  360.2 6.4 %conditional.2 = ((f32[8,256]{1,0:T(8,128)S(1)}, f32[8,256]{1,0:T(8,128)S(1)}, f32[256,8,64]{0,2,1:T(8,128)S(1)})) conditional(s32[]{:T(128)} %convert_element_type.161, (f32[8,256]{1,0:T(8,128)S(1)}, f32[8,256]{1,0:T(8,128)S(1)}, f32[256,8,64]{0,2,1:T(8,128)S(1)}) %tuple.110, (s32[]{:T(128)}, s32[512]{0:T(512)S(1)}, s32[256]{0:T(256)S(1)}, ...), branch_computations={%region_10.10_spmd, %region_11.13_spmd} | conditional | flops 286661120 | bytes 17808462 | solution.py:219
  362.4 1.4 fusion.2
  367.8 6.4 %conditional.2 = ((f32[8,256]{1,0:T(8,128)S(1)}, f32[8,256]{1,0:T(8,128)S(1)}, f32[256,8,64]{0,2,1:T(8,128)S(1)})) conditional(s32[]{:T(128)} %convert_element_type.161, (f32[8,256]{1,0:T(8,128)S(1)}, f32[8,256]{1,0:T(8,128)S(1)}, f32[256,8,64]{0,2,1:T(8,128)S(1)}) %tuple.110, (s32[]{:T(128)}, s32[512]{0:T(512)S(1)}, s32[256]{0:T(256)S(1)}, ...), branch_computations={%region_10.10_spmd, %region_11.13_spmd} | conditional | flops 286661120 | bytes 17808462 | solution.py:219
  370.0 1.4 fusion.2
  375.5 6.4 %conditional.2 = ((f32[8,256]{1,0:T(8,128)S(1)}, f32[8,256]{1,0:T(8,128)S(1)}, f32[256,8,64]{0,2,1:T(8,128)S(1)})) conditional(s32[]{:T(128)} %convert_element_type.161, (f32[8,256]{1,0:T(8,128)S(1)}, f32[8,256]{1,0:T(8,128)S(1)}, f32[256,8,64]{0,2,1:T(8,128)S(1)}) %tuple.110, (s32[]{:T(128)}, s32[512]{0:T(512)S(1)}, s32[256]{0:T(256)S(1)}, ...), branch_computations={%region_10.10_spmd, %region_11.13_spmd} | conditional | flops 286661120 | bytes 17808462 | solution.py:219
  377.6 1.4 fusion.2
  383.1 6.4 %conditional.2 = ((f32[8,256]{1,0:T(8,128)S(1)}, f32[8,256]{1,0:T(8,128)S(1)}, f32[256,8,64]{0,2,1:T(8,128)S(1)})) conditional(s32[]{:T(128)} %convert_element_type.161, (f32[8,256]{1,0:T(8,128)S(1)}, f32[8,256]{1,0:T(8,128)S(1)}, f32[256,8,64]{0,2,1:T(8,128)S(1)}) %tuple.110, (s32[]{:T(128)}, s32[512]{0:T(512)S(1)}, s32[256]{0:T(256)S(1)}, ...), branch_computations={%region_10.10_spmd, %region_11.13_spmd} | conditional | flops 286661120 | bytes 17808462 | solution.py:219
  385.3 1.4 fusion.2
  390.7 6.4 %conditional.2 = ((f32[8,256]{1,0:T(8,128)S(1)}, f32[8,256]{1,0:T(8,128)S(1)}, f32[256,8,64]{0,2,1:T(8,128)S(1)})) conditional(s32[]{:T(128)} %convert_element_type.161, (f32[8,256]{1,0:T(8,128)S(1)}, f32[8,256]{1,0:T(8,128)S(1)}, f32[256,8,64]{0,2,1:T(8,128)S(1)}) %tuple.110, (s32[]{:T(128)}, s32[512]{0:T(512)S(1)}, s32[256]{0:T(256)S(1)}, ...), branch_computations={%region_10.10_spmd, %region_11.13_spmd} | conditional | flops 286661120 | bytes 17808462 | solution.py:219
  392.9 1.4 fusion.2
  398.4 6.4 %conditional.2 = ((f32[8,256]{1,0:T(8,128)S(1)}, f32[8,256]{1,0:T(8,128)S(1)}, f32[256,8,64]{0,2,1:T(8,128)S(1)})) conditional(s32[]{:T(128)} %convert_element_type.161, (f32[8,256]{1,0:T(8,128)S(1)}, f32[8,256]{1,0:T(8,128)S(1)}, f32[256,8,64]{0,2,1:T(8,128)S(1)}) %tuple.110, (s32[]{:T(128)}, s32[512]{0:T(512)S(1)}, s32[256]{0:T(256)S(1)}, ...), branch_computations={%region_10.10_spmd, %region_11.13_spmd} | conditional | flops 286661120 | bytes 17808462 | solution.py:219
  406.0 6.4 %conditional.2 = ((f32[8,256]{1,0:T(8,128)S(1)}, f32[8,256]{1,0:T(8,128)S(1)}, f32[256,8,64]{0,2,1:T(8,128)S(1)})) conditional(s32[]{:T(128)} %convert_element_type.161, (f32[8,256]{1,0:T(8,128)S(1)}, f32[8,256]{1,0:T(8,128)S(1)}, f32[256,8,64]{0,2,1:T(8,128)S(1)}) %tuple.110, (s32[]{:T(128)}, s32[512]{0:T(512)S(1)}, s32[256]{0:T(256)S(1)}, ...), branch_computations={%region_10.10_spmd, %region_11.13_spmd} | conditional | flops 286661120 | bytes 17808462 | solution.py:219
  412.7 3.4 all_gather.28
  416.1 1.5 fusion.38
  (259 shorter events, 99.7 us)
Async XLA Ops:
  6.5 283.5 %copy-start = (bf16[1024,1024]{1,0:T(8,128)(2,1)S(1)}, bf16[1024,1024]{1,0:T(8,128)(2,1)}, u32[]{:S(2)}) copy-start(bf16[1024,1024]{1,0:T(8,128)(2,1)} %param.38) | copy-start | bytes 6291460
  6.5 13.1 %all-gather.5.cloned.1.call-start = ((), (), s32[]{:S(2)}) async-start(), calls=%async_computation.1 | async-start | bytes 1572864 | tf_op jit(solution)/shard_map/all_gather | solution.py:135
  7.3 252.8 %all-gather.9.cloned.1.call-start = ((), (), s32[]{:S(2)}) async-start(), calls=%async_computation.3 | async-start | bytes 2228224 | tf_op jit(solution)/shard_map/all_gather | solution.py:23
  21.1 3.8 copy-start.14
  23.9 3.7 copy-start.4
  28.5 2.9 copy-start.8
  31.2 2.7 copy-start.6
  110.6 5.5 %copy-start.5 = (f32[256,512]{1,0:T(8,128)S(1)}, f32[256,512]{1,0:T(8,128)}, u32[]{:S(2)}) copy-start(f32[256,512]{1,0:T(8,128)} %copy-done.4) | copy-start | bytes 1572868
  110.7 5.5 %copy-start.10 = (f32[256,4]{0,1:T(4,128)S(1)}, f32[256,4]{0,1:T(4,128)}, u32[]{:S(2)}) copy-start(f32[256,4]{0,1:T(4,128)} %param.30) | copy-start | bytes 12292
  116.8 1.3 copy-start.7
  116.8 2.1 copy-start.13
  125.7 165.1 %all-to-all-start = ((bf16[16,256,512]{1,2,0:T(8,128)(2,1)}), bf16[16,256,512]{1,2,0:T(8,128)(2,1)}, u32[]{:S(2)}, u32[]{:S(2)}) async-start(bf16[16,256,512]{1,2,0:T(8,128)(2,1)} %stack.2), calls=%async_computation | async-start | bytes 8388608 | tf_op jit(solution)/shard_map/all_to_all | solution.py:16
  132.1 212.7 %all-gather.7.cloned.1.call-start = ((), (), s32[]{:S(2)}) async-start(), calls=%async_computation.2 | async-start | bytes 4456448 | tf_op jit(solution)/shard_map/all_gather | solution.py:191
  260.0 18.9 %copy-start.2 = (f32[256,4,128]{0,2,1:T(8,128)S(1)}, f32[256,4,128]{0,2,1:T(8,128)}, u32[]{:S(2)}) copy-start(f32[256,4,128]{0,2,1:T(8,128)} %copy.121) | copy-start | bytes 1572868
  278.8 1.8 copy-start.11
  303.6 47.6 %copy-start.9 = (bf16[256,512]{0,1:T(8,128)(2,1)S(1)}, bf16[256,512]{0,1:T(8,128)(2,1)}, u32[]{:S(2)}) copy-start(bf16[256,512]{0,1:T(8,128)(2,1)} %copy.122) | copy-start | bytes 786436
  351.2 61.3 %copy-start.12 = (f32[512]{0:T(512)S(1)}, f32[512]{0:T(512)}, u32[]{:S(2)}) copy-start(f32[512]{0:T(512)} %param.37) | copy-start | bytes 6148
  412.4 3.7 copy-start.3
  412.7 4.9 %copy-start.1 = (bf16[1024,1024]{1,0:T(8,128)(2,1)S(1)}, bf16[1024,1024]{1,0:T(8,128)(2,1)}, u32[]{:S(2)}) copy-start(bf16[1024,1024]{1,0:T(8,128)(2,1)} %param.38) | copy-start | bytes 6291460
Sparse Core Ops, SparseCore 0:
  8.9 10.6 all-gather.4
  111.5 108.8 all-gather.8
  260.1 84.6 all-gather.6
